TPU v7x, 32 devices: a whole 2x2x4 slice. The times are simulated.
32 devices in a mesh: sp: 8 (over z, x), tp: 4 (over y, core).
Axes of the slice: x: 2, y: 2, z: 4, core: 2. Of those that a mesh axis runs over, the one named last changes fastest.
Arguments:
- residual: bfloat16 [2048, 2048], P(('sp', 'tp')), may hold values from -6 to 6
- queries: bfloat16 [2048, 1024], P('sp', 'tp'), may hold values from -8 to 8
- key_pairs: bfloat16 [2048, 512], P('sp', 'tp'), may hold values from -8 to 8
- values: bfloat16 [2048, 512], P('sp', 'tp'), may hold values from -6 to 6
- lambdas: float32 [8], P('tp'), may hold values from 0.3 to 0.8
- head_gain: float32 [128], replicated, may hold values from 0.1 to 1.9
- out_weight: bfloat16 [1024, 2048], replicated, may hold values from -0.1875 to 0.1875
- mixer_gain: float32 [2048], replicated, may hold values from 0.1 to 1.9
- before_gain: float32 [2048], replicated, may hold values from 0.1 to 1.9
- after_gain: float32 [2048], replicated, may hold values from 0.1 to 1.9
- gate_weight: bfloat16 [2048, 5632], P('sp', 'tp'), may hold values from -0.125 to 0.125
- up_weight: bfloat16 [2048, 5632], P('sp', 'tp'), may hold values from -0.125 to 0.125
- down_weight: bfloat16 [5632, 2048], P('tp', 'sp'), may hold values from -0.078125 to 0.078125
Outputs:
- updated: bfloat16 [2048, 2048], P(('sp', 'tp'))
All inputs are finite; a program needn't handle non-finite values.
Results may differ from a plain program's by a relative error of at most 0.014.
Values may be sent and summed in bfloat16 or wider, within the bound.
A program may use at most 128 MiB of HBM per device.

v0:
```python
import math
import jax
import jax.numpy as jnp
from jax import lax
from jax.sharding import PartitionSpec as P

HEAD_DIM = 64


def row_norm(values_in, gain, epsilon):
    mean_square = jnp.mean(values_in * values_in, axis=-1, keepdims=True)
    return values_in * lax.rsqrt(mean_square + epsilon) * gain


def on_device(
    residual,
    queries,
    key_pairs,
    values,
    lambdas,
    head_gain,
    out_weight,
    mixer_gain,
    before_gain,
    after_gain,
    gate_weight,
    up_weight,
    down_weight,
):
    tokens_here = queries.shape[0]
    quarter = residual.shape[0]
    width = 2 * HEAD_DIM
    local_heads = queries.shape[1] // width
    scale = 1.0 / math.sqrt(HEAD_DIM)
    height = local_heads * tokens_here
    query_rows = jnp.transpose(
        queries.reshape(tokens_here, local_heads, 2, HEAD_DIM), (2, 1, 0, 3)
    ).reshape(2, height, HEAD_DIM)
    empty = (
        jnp.full((height,), -1e30, jnp.float32),
        jnp.zeros((height,), jnp.float32),
        jnp.zeros((height, width), jnp.float32),
    )
    state = (empty, empty)
    key_piece = lax.all_gather(key_pairs, "sp", axis=0, tiled=True)
    value_piece = lax.all_gather(values, "sp", axis=0, tiled=True)
    length = key_piece.shape[0]
    span = length
    for split_count in range(1, length + 1):
        if length % split_count == 0 and length // split_count <= 2048:
            span = length // split_count
            break
    key_blocks = key_piece.reshape(length // span, span, 2, HEAD_DIM)
    value_blocks = value_piece.reshape(length // span, span, width)

    def advance(carry, blocks_in):
        key_block, value_block = blocks_in
        renewed = []
        for which in range(2):
            running_top, running_total, running_numer = carry[which]
            score = (
                jnp.dot(
                    query_rows[which], key_block[:, which].T, preferred_element_type=jnp.float32
                )
                * scale
            )
            new_top = jnp.maximum(running_top, jnp.max(score, axis=1))
            shrink = jnp.exp(running_top - new_top)
            expo = jnp.exp(score - new_top[:, None])
            new_total = running_total * shrink + jnp.sum(expo, axis=1)
            new_numer = running_numer * shrink[:, None] + jnp.dot(
                expo.astype(jnp.bfloat16), value_block, preferred_element_type=jnp.float32
            )
            renewed.append((new_top, new_total, new_numer))
        return (tuple(renewed), None)

    state, _ = lax.scan(advance, state, (key_blocks, value_blocks))
    first_map, second_map = state
    lambda_rows = jnp.repeat(lambdas, tokens_here)[:, None]
    attended = first_map[2] / first_map[1][:, None] - lambda_rows * (
        second_map[2] / second_map[1][:, None]
    )
    normed = row_norm(attended, head_gain, 1e-05).astype(jnp.bfloat16)
    head_out = jnp.transpose(normed.reshape(local_heads, tokens_here, width), (1, 0, 2)).reshape(
        tokens_here, local_heads * width
    )
    grouped = head_out.reshape(lax.axis_size("tp"), quarter, local_heads * width)
    mixed = jnp.dot(
        lax.all_to_all(grouped, "tp", split_axis=0, concat_axis=2, tiled=True)[0],
        out_weight,
        preferred_element_type=jnp.float32,
    ).astype(jnp.bfloat16)[None][0]
    stream = residual.astype(jnp.float32) + row_norm(mixed.astype(jnp.float32), mixer_gain, 1e-06)
    normed_in = row_norm(stream, before_gain, 1e-06).astype(jnp.bfloat16)
    gathered = lax.all_gather(normed_in, "tp", axis=0, tiled=True)
    empty_hidden = jnp.zeros((gathered.shape[0], gate_weight.shape[1]), jnp.float32)
    pieces = (
        lax.all_gather(gate_weight, "sp", axis=0, tiled=True),
        lax.all_gather(up_weight, "sp", axis=0, tiled=True),
    )
    columns = lax.slice_in_dim(gathered, 0, pieces[0].shape[0], axis=1)
    gate_part = jnp.dot(columns, pieces[0], preferred_element_type=jnp.float32)
    up_part = jnp.dot(columns, pieces[1], preferred_element_type=jnp.float32)
    gate = empty_hidden + gate_part
    up = empty_hidden + up_part
    down_whole = lax.all_gather(down_weight, "sp", axis=1, tiled=True)
    hidden = (jax.nn.silu(gate) * up).astype(jnp.bfloat16)
    picked = lax.slice_in_dim(hidden, 0, lax.axis_size("tp") * quarter, axis=0)
    channel = lax.psum_scatter(
        jnp.dot(picked, down_whole, preferred_element_type=jnp.float32).astype(jnp.bfloat16),
        "tp",
        scatter_dimension=0,
        tiled=True,
    )
    updated = stream + 0.5 * row_norm(channel.astype(jnp.float32), after_gain, 1e-06)
    return updated.astype(jnp.bfloat16)


def solution(mesh):
    return jax.shard_map(
        on_device,
        mesh=mesh,
        in_specs=(
            P(("sp", "tp"), None),
            P("sp", "tp"),
            P("sp", "tp"),
            P("sp", "tp"),
            P("tp"),
            P(),
            P(),
            P(),
            P(),
            P(),
            P("sp", "tp"),
            P("sp", "tp"),
            P("tp", "sp"),
        ),
        out_specs=P(("sp", "tp"), None),
        check_vma=False,
    )
```

profile of v0, /device:TPU:0, one launch (start us, length us, event | category | flops | bytes accessed | tf_op | source)
XLA Modules:
  0.0 430.2 jit_solution(3633528644462433819)
XLA Ops:
  6.5 0.9 copy.16
  7.5 33.0 %all_gather.18 = bf16[2048,128]{0,1:T(8,128)(2,1)S(1)} all-gather(bf16[256,128]{0,1:T(8,128)(2,1)S(1)} %copy.16), channel_id=1, replica_groups=mesh['sp'=8,'tp'=4] {'sp'}, dimensions={0}, use_global_device_ids=true | all-gather | bytes 589824 | tf_op jit(solution)/shard_map/all_gather | solution.py:45
  40.5 1.0 copy.14
  41.7 0.8 multiply_reduce_fusion.1
  42.5 0.8 fusion
  43.3 31.3 %all_gather.19 = bf16[2048,128]{1,0:T(8,128)(2,1)S(1)} all-gather(bf16[256,128]{1,0:T(8,128)(2,1)S(1)} %copy-done.3), channel_id=1, replica_groups=mesh['sp'=8,'tp'=4] {'sp'}, dimensions={0}, use_global_device_ids=true | all-gather | bytes 589824 | tf_op jit(solution)/shard_map/all_gather | solution.py:46
  74.7 0.8 multiply_reduce_fusion
  75.5 0.8 fusion.2
  76.5 0.9 fusion.29
  77.4 1.5 multiply_reduce_fusion.4
  79.3 7.2 %all_to_all.15 = bf16[4,64,256]{2,1,0:T(8,128)(2,1)S(1)} all-to-all(bf16[4,64,256]{2,1,0:T(8,128)(2,1)S(1)} %reshape_reshape.3), channel_id=1, replica_groups=mesh['sp'=8,'tp'=4] {'tp'}, dimensions={0} | all-to-all | bytes 262144 | tf_op jit(solution)/shard_map/all_to_all | solution.py:89
  86.6 3.1 multiply_reduce_fusion.3
  90.1 0.9 multiply_convert_fusion
  91.0 0.7 all-gather.7.cloned.1.call-update
  91.8 0.7 all-gather.11.cloned.1.call-update
  93.1 15.0 %all-gather.5.cloned.1.call-done = bf16[256,2048]{1,0:T(8,128)(2,1)} async-done(((bf16[64,2048]{1,0:T(8,128)(2,1)}), bf16[256,2048]{1,0:T(8,128)(2,1)}) %all-gather.5.cloned.1.call-update) | async-done | bytes 1048592 | tf_op jit(solution)/shard_map/all_gather | solution.py:95
  108.1 94.5 %all-gather.7.cloned.1.call-done = bf16[2048,1408]{1,0:T(8,128)(2,1)} async-done(((bf16[256,1408]{1,0:T(8,128)(2,1)}), bf16[2048,1408]{1,0:T(8,128)(2,1)}) %all-gather.7.cloned.1.call-update) | async-done | bytes 5767184 | tf_op jit(solution)/shard_map/all_gather | solution.py:98
  202.6 4.8 %fusion.45 = f32[256,1408]{1,0:T(8,128)S(1)} fusion(bf16[256,2048]{1,0:T(8,128)(2,1)} %all-gather.5.cloned.1.call-done, bf16[2048,1408]{1,0:T(8,128)(2,1)} %all-gather.7.cloned.1.call-done), kind=kOutput, calls=%fused_computation.58 | convolution fusion | flops 1476395008 | bytes 8257536 | tf_op jit(solution)/shard_map/dot_general | solution.py:102
  207.4 88.6 %all-gather.11.cloned.1.call-done = bf16[1408,2048]{1,0:T(8,128)(2,1)} async-done(((bf16[1408,256]{1,0:T(8,128)(2,1)}), bf16[1408,2048]{1,0:T(8,128)(2,1)}) %all-gather.11.cloned.1.call-update) | async-done | bytes 5767184 | tf_op jit(solution)/shard_map/all_gather | solution.py:106
  296.0 92.6 %all-gather.9.cloned.1.call-done = bf16[2048,1408]{1,0:T(8,128)(2,1)} async-done(((bf16[256,1408]{1,0:T(8,128)(2,1)}), bf16[2048,1408]{1,0:T(8,128)(2,1)}) %all-gather.9.cloned.1.call-update) | async-done | bytes 5767184 | tf_op jit(solution)/shard_map/all_gather | solution.py:99
  388.6 8.9 %convolution_convert_fusion = bf16[256,2048]{1,0:T(8,128)(2,1)} fusion(bf16[1408,2048]{1,0:T(8,128)(2,1)} %all-gather.11.cloned.1.call-done, bf16[256,2048]{1,0:T(8,128)(2,1)S(1)} %copy-done.7, bf16[2048,1408]{1,0:T(8,128)(2,1)} %all-gather.9.cloned.1.call-done, f32[256,1408]{1,0:T(8,128)S(1)} %fusion.45), kind=kOutput, calls=%fused_computation.10 | convolution fusion | flops 2955476992 | bytes 15073280 | tf_op jit(solution)/shard_map/dot_general | solution.py:110
  397.5 23.1 %reduce-scatter.2.cloned.1.call-done = bf16[64,2048]{1,0:T(8,128)(2,1)} async-done(((bf16[256,2048]{1,0:T(8,128)(2,1)}), bf16[64,2048]{1,0:T(8,128)(2,1)}) %reduce-scatter.2.cloned.1.call-update) | async-done | bytes 262160 | tf_op jit(solution)/shard_map/reduce_scatter | solution.py:109
  420.6 1.1 fusion.32
  421.7 1.9 fusion.36
  (45 shorter events, 1.8 us)
Async XLA Ops:
  6.5 69.8 %copy-start = (f32[2]{0:T(128)S(1)}, f32[2]{0:T(128)}, u32[]{:S(2)}) copy-start(f32[2]{0:T(128)} %param.17) | copy-start | bytes 28
  6.5 101.6 %all-gather.5.cloned.1.call-start = ((), (), s32[]{:S(2)}) async-start(), calls=%async_computation.2 | async-start | bytes 1310720 | tf_op jit(solution)/shard_map/all_gather | solution.py:95
  41.7 1.7 copy-start.3
  77.3 1.6 copy-start.6
  78.8 10.9 %copy-start.1 = (bf16[64,2048]{1,0:T(8,128)(2,1)S(1)}, bf16[64,2048]{1,0:T(8,128)(2,1)}, u32[]{:S(2)}) copy-start(bf16[64,2048]{1,0:T(8,128)(2,1)} %param.13) | copy-start | bytes 786436
  78.9 10.9 %copy-start.2 = (f32[2048]{0:T(1024)S(1)}, f32[2048]{0:T(1024)}, u32[]{:S(2)}) copy-start(f32[2048]{0:T(1024)} %param.20) | copy-start | bytes 24580
  78.9 11.2 %copy-start.4 = (f32[2048]{0:T(1024)S(1)}, f32[2048]{0:T(1024)}, u32[]{:S(2)}) copy-start(f32[2048]{0:T(1024)} %param.21) | copy-start | bytes 24580
  91.0 111.6 %all-gather.7.cloned.1.call-start = ((), (), s32[]{:S(2)}) async-start(), calls=%async_computation.3 | async-start | bytes 6488064 | tf_op jit(solution)/shard_map/all_gather | solution.py:98
  91.8 204.3 %all-gather.11.cloned.1.call-start = ((), (), s32[]{:S(2)}) async-start(), calls=%async_computation.5 | async-start | bytes 6488064 | tf_op jit(solution)/shard_map/all_gather | solution.py:106
  92.5 296.1 %all-gather.9.cloned.1.call-start = ((), (), s32[]{:S(2)}) async-start(), calls=%async_computation.4 | async-start | bytes 6488064 | tf_op jit(solution)/shard_map/all_gather | solution.py:99
  93.1 327.5 %reduce-scatter.2.cloned.1.call-start = ((), (), s32[]{:S(2)}) async-start(), calls=%async_computation.6 | async-start | bytes 1310720 | tf_op jit(solution)/shard_map/reduce_scatter | solution.py:109
  108.1 280.5 %copy-start.7 = (bf16[256,2048]{1,0:T(8,128)(2,1)S(1)}, bf16[256,2048]{1,0:T(8,128)(2,1)}, u32[]{:S(2)}) copy-start(bf16[256,2048]{1,0:T(8,128)(2,1)} %all-gather.5.cloned.1.call-done) | copy-start | bytes 3145732
  207.4 214.3 %copy-start.5 = (f32[2048]{0:T(1024)S(1)}, f32[2048]{0:T(1024)}, u32[]{:S(2)}) copy-start(f32[2048]{0:T(1024)} %param.22) | copy-start | bytes 24580
Sparse Core Ops, SparseCore 0:
  91.1 16.9 all-gather.4
  110.3 92.2 all-gather.6
  204.7 91.2 all-gather.10
  298.1 90.4 all-gather.8
  397.6 22.9 reduce-scatter.1
where the time goes:
time: 431 us; the launch traced here: 430 us
  waiting for transfers between devices  316 us (73%)
  blocking collectives  71.5 us (17%)
  matrix products  20.8 us (5%)
  between operations  13.4 us (3%)
  other arithmetic  6.02 us (1%)
    all_gather x1, waiting for transfers between devices, on_device(): lax.all_gather(gate_weight, 'sp', axis=0, tiled=True)  94.5 us
    all_gather x1, waiting for transfers between devices, on_device(): lax.all_gather(up_weight, 'sp', axis=0, tiled=True)  92.6 us
    all_gather x1, waiting for transfers between devices, on_device(): down_whole = lax.all_gather(down_weight, 'sp', axis=1, tiled=True)  88.6 us
    all_gather x1, blocking collectives, on_device(): key_piece = lax.all_gather(key_pairs, 'sp', axis=0, tiled=True)  33 us
    all_gather x1, blocking collectives, on_device(): value_piece = lax.all_gather(values, 'sp', axis=0, tiled=True)  31.3 us
    reduce_scatter x1, waiting for transfers between devices, on_device(): lax.psum_scatter(jnp.dot(picked, down_whole, preferred_element_type=jnp.f...  23.1 us
    all_gather x1, waiting for transfers between devices, on_device(): gathered = lax.all_gather(normed_in, 'tp', axis=0, tiled=True)  15 us
    dot_general x1, matrix products, on_device(): jnp.dot(picked, down_whole, preferred_element_type=jnp.float32)  8.9 us
  transfers between devices with their start and end apart: 5, of which 5 were waited for; matrix products, arithmetic and copies ran while one was open for 1% of the time, Pallas kernels for 0%

commit v1 on v0

--- a/solution.py
+++ b/solution.py
@@ -103,7 +103,12 @@
     up_part = jnp.dot(columns, pieces[1], preferred_element_type=jnp.float32)
     gate = empty_hidden + gate_part
     up = empty_hidden + up_part
-    down_whole = lax.all_gather(down_weight, "sp", axis=1, tiled=True)
+    ring = [down_weight]
+    for hop in range(7):
+        ring.append(lax.ppermute(ring[-1], "sp", [(dev, (dev + 1) % 8) for dev in range(8)]))
+    down_whole = jnp.roll(
+        jnp.concatenate(ring[::-1], axis=1), (lax.axis_index("sp") + 1) * ring[0].shape[1], axis=1
+    )
     hidden = (jax.nn.silu(gate) * up).astype(jnp.bfloat16)
     picked = lax.slice_in_dim(hidden, 0, lax.axis_size("tp") * quarter, axis=0)
     channel = lax.psum_scatter(

time: 431 us -> 408 us (0.947)
  waiting for transfers between devices: 316 us -> 265 us
  local copies, waits for them, and re-layouts: 2.59 us -> 26.7 us
    ppermute x0 -> x7, waiting for transfers between devices: none -> 207 us  [on_device(): lax.ppermute(ring[-1], 'sp', [(dev, (dev + 1) % 8) for dev in range(8)])]
    all_gather x1, waiting for transfers between devices: 94.5 us -> 0.01 us  [on_device(): lax.all_gather(gate_weight, 'sp', axis=0, tiled=True)]
    all_gather x1 -> x0, waiting for transfers between devices: 88.6 us -> none  [on_device(): down_whole = lax.all_gather(down_weight, 'sp', axis=1, tiled=True)]
    all_gather x1, waiting for transfers between devices: 92.6 us -> 33.9 us  [on_device(): lax.all_gather(up_weight, 'sp', axis=0, tiled=True)]
    unnamed x23 -> x48, local copies, waits for them, and re-layouts: 2.11 us -> 25.2 us
    all_gather x1, waiting for transfers between devices: 15 us -> 0.01 us  [on_device(): gathered = lax.all_gather(normed_in, 'tp', axis=0, tiled=True)]
  transfers between devices with their start and end apart: 5 -> 11, of which waited for: 5 -> 9; matrix products, arithmetic and copies ran while one was open for 1% -> 7% of each run, Pallas kernels for 0% -> 0%
where the time goes in v1:
time: 408 us; the launch traced here: 407 us
  waiting for transfers between devices  265 us (65%)
  blocking collectives  71.8 us (18%)
  local copies, waits for them, and re-layouts  26.7 us (7%)
  matrix products  22.3 us (5%)
  between operations  13.4 us (3%)
  other arithmetic  6.02 us (1%)
    ppermute x7, waiting for transfers between devices, on_device(): lax.ppermute(ring[-1], 'sp', [(dev, (dev + 1) % 8) for dev in range(8)])  207 us
    all_gather x1, waiting for transfers between devices, on_device(): lax.all_gather(up_weight, 'sp', axis=0, tiled=True)  33.9 us
    all_gather x1, blocking collectives, on_device(): value_piece = lax.all_gather(values, 'sp', axis=0, tiled=True)  33.4 us
    all_gather x1, blocking collectives, on_device(): key_piece = lax.all_gather(key_pairs, 'sp', axis=0, tiled=True)  31.2 us
    unnamed x48, local copies, waits for them, and re-layouts  25.2 us
    reduce_scatter x1, waiting for transfers between devices, on_device(): lax.psum_scatter(jnp.dot(picked, down_whole, preferred_element_type=jnp.f...  23.2 us
    dot_general x1, matrix products, on_device(): jnp.dot(picked, down_whole, preferred_element_type=jnp.float32)  9.22 us
  transfers between devices with their start and end apart: 11, of which 9 were waited for; matrix products, arithmetic and copies ran while one was open for 7% of the time, Pallas kernels for 0%

profile of v1, /device:TPU:0, one launch (start us, length us, event | category | flops | bytes accessed | tf_op | source)
XLA Modules:
  0.0 407.3 jit_solution(9847988821750489172)
XLA Ops:
  6.5 33.4 %all_gather.16 = bf16[2048,128]{1,0:T(8,128)(2,1)S(1)} all-gather(bf16[256,128]{1,0:T(8,128)(2,1)} %param.16), channel_id=1, replica_groups=mesh['sp'=8,'tp'=4] {'sp'}, dimensions={0}, use_global_device_ids=true | all-gather | bytes 589824 | tf_op jit(solution)/shard_map/all_gather | solution.py:46
  42.0 31.2 %all_gather.15 = bf16[2048,128]{0,1:T(8,128)(2,1)S(1)} all-gather(bf16[256,128]{0,1:T(8,128)(2,1)S(1)} %copy.16), channel_id=1, replica_groups=mesh['sp'=8,'tp'=4] {'sp'}, dimensions={0}, use_global_device_ids=true | all-gather | bytes 589824 | tf_op jit(solution)/shard_map/all_gather | solution.py:45
  77.7 1.5 multiply_reduce_fusion.4
  79.6 7.2 %all_to_all.15 = bf16[4,64,256]{2,1,0:T(8,128)(2,1)S(1)} all-to-all(bf16[4,64,256]{2,1,0:T(8,128)(2,1)S(1)} %reshape_reshape.3), channel_id=1, replica_groups=mesh['sp'=8,'tp'=4] {'tp'}, dimensions={0} | all-to-all | bytes 262144 | tf_op jit(solution)/shard_map/all_to_all | solution.py:89
  86.9 3.1 multiply_reduce_fusion.3
  92.8 1.9 collective-permute-start
  94.7 18.5 %collective-permute-done = bf16[1408,256]{1,0:T(8,128)(2,1)S(1)} collective-permute-done((bf16[1408,256]{1,0:T(8,128)(2,1)S(1)}, bf16[1408,256]{1,0:T(8,128)(2,1)S(1)}, u32[]{:S(2)}, u32[]{:S(2)}) %collective-permute-start) | collective-permute-done | bytes 720928 | tf_op jit(solution)/shard_map/ppermute | solution.py:108
  113.2 30.2 %collective-permute-done.1 = bf16[1408,256]{1,0:T(8,128)(2,1)S(1)} collective-permute-done((bf16[1408,256]{1,0:T(8,128)(2,1)S(1)}, bf16[1408,256]{1,0:T(8,128)(2,1)S(1)}, u32[]{:S(2)}, u32[]{:S(2)}) %collective-permute-start.1) | collective-permute-done | bytes 720928 | tf_op jit(solution)/shard_map/ppermute | solution.py:108
  143.4 28.0 %collective-permute-done.2 = bf16[1408,256]{1,0:T(8,128)(2,1)S(1)} collective-permute-done((bf16[1408,256]{1,0:T(8,128)(2,1)S(1)}, bf16[1408,256]{1,0:T(8,128)(2,1)S(1)}, u32[]{:S(2)}, u32[]{:S(2)}) %collective-permute-start.2) | collective-permute-done | bytes 720928 | tf_op jit(solution)/shard_map/ppermute | solution.py:108
  171.4 35.6 %collective-permute-done.3 = bf16[1408,256]{1,0:T(8,128)(2,1)S(1)} collective-permute-done((bf16[1408,256]{1,0:T(8,128)(2,1)S(1)}, bf16[1408,256]{1,0:T(8,128)(2,1)S(1)}, u32[]{:S(2)}, u32[]{:S(2)}) %collective-permute-start.3) | collective-permute-done | bytes 720928 | tf_op jit(solution)/shard_map/ppermute | solution.py:108
  207.9 35.3 %collective-permute-done.4 = bf16[1408,256]{1,0:T(8,128)(2,1)S(1)} collective-permute-done((bf16[1408,256]{1,0:T(8,128)(2,1)S(1)}, bf16[1408,256]{1,0:T(8,128)(2,1)S(1)}, u32[]{:S(2)}, u32[]{:S(2)}) %collective-permute-start.4) | collective-permute-done | bytes 720928 | tf_op jit(solution)/shard_map/ppermute | solution.py:108
  244.0 23.2 %collective-permute-done.5 = bf16[1408,256]{1,0:T(8,128)(2,1)} collective-permute-done((bf16[1408,256]{1,0:T(8,128)(2,1)S(1)}, bf16[1408,256]{1,0:T(8,128)(2,1)}, u32[]{:S(2)}, u32[]{:S(2)}) %collective-permute-start.5) | collective-permute-done | bytes 720928 | tf_op jit(solution)/shard_map/ppermute | solution.py:108
  267.2 35.9 %collective-permute-done.6 = bf16[1408,256]{1,0:T(8,128)(2,1)} collective-permute-done((bf16[1408,256]{1,0:T(8,128)(2,1)}, bf16[1408,256]{1,0:T(8,128)(2,1)}, u32[]{:S(2)}, u32[]{:S(2)}) %collective-permute-start.6) | collective-permute-done | bytes 720928 | tf_op jit(solution)/shard_map/ppermute | solution.py:108
  303.1 2.1 constant_dynamic-update-slice_fusion.15
  305.2 2.1 constant_dynamic-update-slice_fusion.14
  307.2 2.1 constant_dynamic-update-slice_fusion.13
  309.4 2.2 constant_dynamic-update-slice_fusion.12
  315.4 2.1 constant_dynamic-update-slice_fusion.7
  317.4 2.1 constant_dynamic-update-slice_fusion.6
  325.5 5.9 %fusion.51 = f32[256,1408]{1,0:T(8,128)} fusion(bf16[256,2048]{1,0:T(8,128)(2,1)} %all-gather.4.cloned.1.call-done, bf16[2048,1408]{1,0:T(8,128)(2,1)} %all-gather.6.cloned.1.call-done), kind=kOutput, calls=%fused_computation.77 | convolution fusion | flops 1476395008 | bytes 8257536 | tf_op jit(solution)/shard_map/dot_general | solution.py:102
  331.4 33.9 %all-gather.8.cloned.1.call-done = bf16[2048,1408]{1,0:T(8,128)(2,1)} async-done(((bf16[256,1408]{1,0:T(8,128)(2,1)}), bf16[2048,1408]{1,0:T(8,128)(2,1)}) %all-gather.8.cloned.1.call-update) | async-done | bytes 5767184 | tf_op jit(solution)/shard_map/all_gather | solution.py:99
  365.3 9.2 %fusion.7 = bf16[256,2048]{1,0:T(8,128)(2,1)} fusion(bf16[1408,4096]{1,0:T(8,128)(2,1)} %constant_dynamic-update-slice_fusion, s32[]{:T(128)S(6)} %select_n.14, bf16[256,2048]{1,0:T(8,128)(2,1)S(1)} %copy-done.12, bf16[2048,1408]{1,0:T(8,128)(2,1)} %all-gather.8.cloned.1.call-done, f32[256,1408]{1,0:T(8,128)} %fusion.51), kind=kOutput, calls=%fused_computation.12 | convolution fusion | flops 2955476992 | bytes 15073284 | tf_op jit(solution)/shard_map/dot_general | solution.py:115
  374.6 23.2 %reduce-scatter.2.cloned.1.call-done = bf16[64,2048]{1,0:T(8,128)(2,1)} async-done(((bf16[256,2048]{1,0:T(8,128)(2,1)}), bf16[64,2048]{1,0:T(8,128)(2,1)}) %reduce-scatter.2.cloned.1.call-update) | async-done | bytes 262160 | tf_op jit(solution)/shard_map/reduce_scatter | solution.py:114
  398.9 1.9 fusion.41
  (82 shorter events, 22.3 us)
Async XLA Ops:
  6.5 70.1 %copy-start = (f32[2]{0:T(128)S(1)}, f32[2]{0:T(128)}, u32[]{:S(2)}) copy-start(f32[2]{0:T(128)} %param.17) | copy-start | bytes 28
  6.5 318.9 %all-gather.4.cloned.1.call-start = ((), (), s32[]{:S(2)}) async-start(), calls=%async_computation.2 | async-start | bytes 1310720 | tf_op jit(solution)/shard_map/all_gather | solution.py:95
  76.7 2.5 copy-start.11
  77.6 12.4 %copy-start.6 = (bf16[64,2048]{1,0:T(8,128)(2,1)S(1)}, bf16[64,2048]{1,0:T(8,128)(2,1)}, u32[]{:S(2)}) copy-start(bf16[64,2048]{1,0:T(8,128)(2,1)} %param.13) | copy-start | bytes 786436
  77.7 12.4 %copy-start.8 = (f32[2048]{0:T(1024)S(1)}, f32[2048]{0:T(1024)}, u32[]{:S(2)}) copy-start(f32[2048]{0:T(1024)} %param.20) | copy-start | bytes 24580
  77.7 12.7 %copy-start.9 = (f32[2048]{0:T(1024)S(1)}, f32[2048]{0:T(1024)}, u32[]{:S(2)}) copy-start(f32[2048]{0:T(1024)} %param.21) | copy-start | bytes 24580
  79.2 13.6 %copy-start.1 = (bf16[1408,256]{1,0:T(8,128)(2,1)S(1)}, bf16[1408,256]{1,0:T(8,128)(2,1)}, u32[]{:S(2)}) copy-start(bf16[1408,256]{1,0:T(8,128)(2,1)} %param.25) | copy-start | bytes 2162692
  91.3 234.2 %all-gather.6.cloned.1.call-start = ((), (), s32[]{:S(2)}) async-start(), calls=%async_computation.3 | async-start | bytes 6488064 | tf_op jit(solution)/shard_map/all_gather | solution.py:98
  92.0 273.3 %all-gather.8.cloned.1.call-start = ((), (), s32[]{:S(2)}) async-start(), calls=%async_computation.4 | async-start | bytes 6488064 | tf_op jit(solution)/shard_map/all_gather | solution.py:99
  92.8 305.0 %reduce-scatter.2.cloned.1.call-start = ((), (), s32[]{:S(2)}) async-start(), calls=%async_computation.5 | async-start | bytes 1310720 | tf_op jit(solution)/shard_map/reduce_scatter | solution.py:114
  92.8 20.4 %collective-permute-start = (bf16[1408,256]{1,0:T(8,128)(2,1)S(1)}, bf16[1408,256]{1,0:T(8,128)(2,1)S(1)}, u32[]{:S(2)}, u32[]{:S(2)}) collective-permute-start(bf16[1408,256]{1,0:T(8,128)(2,1)S(1)} %copy-done.1), channel_id=1, source_target_pairs={{0,4},{4,8},{8,12},{12,16},{16,20},{20,24},{24,28},{28,0},{1,5},{5... | collective-permute-start | bytes 2162696 | tf_op jit(solution)/shard_map/ppermute | solution.py:108
  113.2 30.2 %collective-permute-start.1 = (bf16[1408,256]{1,0:T(8,128)(2,1)S(1)}, bf16[1408,256]{1,0:T(8,128)(2,1)S(1)}, u32[]{:S(2)}, u32[]{:S(2)}) collective-permute-start(bf16[1408,256]{1,0:T(8,128)(2,1)S(1)} %collective-permute-done), channel_id=1, source_target_pairs={{0,4},{4,8},{8,12},{12,16},{16,20},{20,24},{24,28},{28,0},{1,5},{5... | collective-permute-start | bytes 2162696 | tf_op jit(solution)/shard_map/ppermute | solution.py:108
  143.4 28.0 %collective-permute-start.2 = (bf16[1408,256]{1,0:T(8,128)(2,1)S(1)}, bf16[1408,256]{1,0:T(8,128)(2,1)S(1)}, u32[]{:S(2)}, u32[]{:S(2)}) collective-permute-start(bf16[1408,256]{1,0:T(8,128)(2,1)S(1)} %collective-permute-done.1), channel_id=1, source_target_pairs={{0,4},{4,8},{8,12},{12,16},{16,20},{20,24},{24,28},{28,0},{1,5},{5... | collective-permute-start | bytes 2162696 | tf_op jit(solution)/shard_map/ppermute | solution.py:108
  171.4 35.6 %collective-permute-start.3 = (bf16[1408,256]{1,0:T(8,128)(2,1)S(1)}, bf16[1408,256]{1,0:T(8,128)(2,1)S(1)}, u32[]{:S(2)}, u32[]{:S(2)}) collective-permute-start(bf16[1408,256]{1,0:T(8,128)(2,1)S(1)} %collective-permute-done.2), channel_id=1, source_target_pairs={{0,4},{4,8},{8,12},{12,16},{16,20},{20,24},{24,28},{28,0},{1,5},{5... | collective-permute-start | bytes 2162696 | tf_op jit(solution)/shard_map/ppermute | solution.py:108
  207.0 0.9 copy-start.2
  207.9 35.3 %collective-permute-start.4 = (bf16[1408,256]{1,0:T(8,128)(2,1)S(1)}, bf16[1408,256]{1,0:T(8,128)(2,1)S(1)}, u32[]{:S(2)}, u32[]{:S(2)}) collective-permute-start(bf16[1408,256]{1,0:T(8,128)(2,1)S(1)} %collective-permute-done.3), channel_id=1, source_target_pairs={{0,4},{4,8},{8,12},{12,16},{16,20},{20,24},{24,28},{28,0},{1,5},{5... | collective-permute-start | bytes 2162696 | tf_op jit(solution)/shard_map/ppermute | solution.py:108
  243.2 0.9 copy-start.4
  244.0 23.2 %collective-permute-start.5 = (bf16[1408,256]{1,0:T(8,128)(2,1)S(1)}, bf16[1408,256]{1,0:T(8,128)(2,1)}, u32[]{:S(2)}, u32[]{:S(2)}) collective-permute-start(bf16[1408,256]{1,0:T(8,128)(2,1)S(1)} %collective-permute-done.4), channel_id=1, source_target_pairs={{0,4},{4,8},{8,12},{12,16},{16,20},{20,24},{24,28},{28,0},{1,5},{5... | collective-permute-start | bytes 2162696 | tf_op jit(solution)/shard_map/ppermute | solution.py:108
  267.2 35.9 %collective-permute-start.6 = (bf16[1408,256]{1,0:T(8,128)(2,1)}, bf16[1408,256]{1,0:T(8,128)(2,1)}, u32[]{:S(2)}, u32[]{:S(2)}) collective-permute-start(bf16[1408,256]{1,0:T(8,128)(2,1)} %collective-permute-done.5), channel_id=1, source_target_pairs={{0,4},{4,8},{8,12},{12,16},{16,20},{20,24},{24,28},{28,0},{1,5},{5... | collective-permute-start | bytes 2162696 | tf_op jit(solution)/shard_map/ppermute | solution.py:108
  307.2 12.3 %copy-start.5 = (bf16[1408,256]{1,0:T(8,128)(2,1)S(1)}, bf16[1408,256]{1,0:T(8,128)(2,1)}, u32[]{:S(2)}) copy-start(bf16[1408,256]{1,0:T(8,128)(2,1)} %copy-done.4) | copy-start | bytes 2162692
  309.4 11.2 %copy-start.3 = (bf16[1408,256]{1,0:T(8,128)(2,1)S(1)}, bf16[1408,256]{1,0:T(8,128)(2,1)}, u32[]{:S(2)}) copy-start(bf16[1408,256]{1,0:T(8,128)(2,1)} %copy-done.2) | copy-start | bytes 2162692
  325.5 39.9 %copy-start.12 = (bf16[256,2048]{1,0:T(8,128)(2,1)S(1)}, bf16[256,2048]{1,0:T(8,128)(2,1)}, u32[]{:S(2)}) copy-start(bf16[256,2048]{1,0:T(8,128)(2,1)} %all-gather.4.cloned.1.call-done) | copy-start | bytes 3145732
  331.4 67.4 %copy-start.7 = (bf16[64,2048]{1,0:T(8,128)(2,1)S(1)}, bf16[64,2048]{1,0:T(8,128)(2,1)}, u32[]{:S(2)}) copy-start(bf16[64,2048]{1,0:T(8,128)(2,1)} %param.13) | copy-start | bytes 786436
  331.4 67.5 %copy-start.10 = (f32[2048]{0:T(1024)S(1)}, f32[2048]{0:T(1024)}, u32[]{:S(2)}) copy-start(f32[2048]{0:T(1024)} %param.22) | copy-start | bytes 24580
Sparse Core Ops, SparseCore 0:
  91.4 17.0 all-gather.3
  110.6 133.1 all-gather.5
  246.1 119.2 all-gather.7
  374.7 22.9 reduce-scatter.1
